TPU v7x, 128 devices: a whole 4x4x4 slice. The times are simulated.
128 devices in a mesh: sp: 16 (over z, y), dp: 8 (over x, core).
Axes of the slice: x: 4, y: 4, z: 4, core: 2. Of those that a mesh axis runs over, the one named last changes fastest.
Arguments:
- layer_input: bfloat16 [8, 2048, 2048], P('dp', 'sp'), may hold values from -0.0390625 to 0.0390625
- queries: bfloat16 [8, 2048, 2048], P('dp', 'sp'), may hold values from -6 to 6
- key_vectors: bfloat16 [8, 2048, 2048], P('dp', 'sp'), may hold values from -6 to 6
- values: bfloat16 [8, 2048, 4096], P('dp', 'sp'), may hold values from -6 to 6
- cotangent: bfloat16 [8, 2048, 4096], P('dp', 'sp'), may hold values from -0.3125 to 0.3125
- log_decay: float32 [8, 16, 2048], P('dp', 'sp'), may hold values from -3 to 0
- key_weight: bfloat16 [2048, 2048], P('dp'), may hold values from -0.125 to 0.125
Outputs:
- grad_query: bfloat16 [8, 2048, 2048], P('dp', 'sp')
- grad_value: bfloat16 [8, 2048, 4096], P('dp', 'sp')
- grad_input: bfloat16 [8, 2048, 2048], P('dp', 'sp')
- grad_key_weight: float32 [2048, 2048], P('dp')
All inputs are finite; a program needn't handle non-finite values.
Results may differ from a plain program's by a relative error of at most 0.012.
Values may be sent and summed in bfloat16 or wider, within the bound.
A program may use at most 128 MiB of HBM per device.

v0:
```python
import functools

import jax
import jax.numpy as jnp
from jax import lax
from jax.experimental import pallas as pl
from jax.experimental.pallas import tpu as pltpu
from jax.sharding import PartitionSpec as P

F32 = jnp.float32
BF16 = jnp.bfloat16
SP, DPN = 16, 8
GROUP = 8
DK, DV, D = 256, 512, 2048
BLOCK = 128
MESH = pl.DeviceIdType.MESH


def dot(a, b, ca, cb, precision=None):
    return lax.dot_general(
        a, b, (((ca,), (cb,)), ((), ())), preferred_element_type=F32, precision=precision
    )


def lanes(scale, width):
    return jnp.concatenate([scale] * (width // 128), axis=1)


def kernel(
    x_ref, q_ref, k_ref, v_ref, g_ref, lam_ref, w_ref,
    dq_ref, dv_ref, dx_ref, dw_ref,
    rq, rk, rv, rg, rlam, w_all, x_all,
    qs, ks, ee, tails, wgt,
    acc_q, acc_k, acc_v, m_st, g_st, st_tx, st_rx,
    out_q, out_k, out_v, dk_all, dx_st, dw_acc, dw_tx, dw_rx, sum_tx, sum_rx,
    in_send, in_recv, lam_send, lam_recv, x_send, x_recv, w_sem,
    st_send, st_recv, out_send, out_recv, dk_send, dk_fwd, dk_recv,
    dx_send, dx_recv, rs_send, rs_recv, ag_send, ag_recv,
):
    s = lax.axis_index("sp")
    d = lax.axis_index("dp")
    gz = s // GROUP
    me = s % GROUP
    head = (me + 4 * gz) % GROUP
    base = GROUP * gz
    partner = GROUP * (1 - gz) + (head + 4 * (1 - gz)) % GROUP
    xi, core = d // 2, d % 2
    sibling = 2 * xi + 1 - core

    def col(i, width):
        return pl.ds(pl.multiple_of(i * width, width), width)

    def remote(src, dst, ssem, rsem, to):
        return pltpu.make_async_remote_copy(
            src_ref=src, dst_ref=dst, send_sem=ssem, recv_sem=rsem,
            device_id=to, device_id_type=MESH,
        )

    def arrived(dst, sem):
        pltpu.make_async_copy(dst, dst, sem).wait()

    barrier = pltpu.get_barrier_semaphore()

    @pl.loop(1, SP)
    def _(i):
        pl.semaphore_signal(barrier, inc=1, device_id=((s + i) % SP, d), device_id_type=MESH)

    @pl.loop(1, DPN)
    def _(i):
        pl.semaphore_signal(barrier, inc=1, device_id=(s, (d + i) % DPN), device_id_type=MESH)

    pl.semaphore_wait(barrier, SP + DPN - 2)

    lam_to = [s // 2, GROUP + (s // 2 + 4) % GROUP]
    for half in range(2):
        src = lam_ref.at[pl.ds(8 * half, 8), :]

        @pl.when(lam_to[half] == s)
        def _():
            pltpu.make_async_copy(src, rlam.at[s % 2], lam_recv.at[s % 2]).start()

        @pl.when(lam_to[half] != s)
        def _():
            remote(src, rlam.at[s % 2], lam_send.at[half], lam_recv.at[s % 2], (lam_to[half], d)).start()

    pairs = ((q_ref, rq, DK), (k_ref, rk, DK), (v_ref, rv, DV), (g_ref, rg, DV))
    for n, (src, dst, width) in enumerate(pairs):
        pltpu.make_async_copy(src.at[:, col(head, width)], dst.at[me], in_recv.at[n, me]).start()

    @pl.loop(1, GROUP)
    def _(i):
        to = (me + i) % GROUP
        its_head = (to + 4 * gz) % GROUP
        for n, (src, dst, width) in enumerate(pairs):
            remote(
                src.at[:, col(its_head, width)], dst.at[me],
                in_send.at[n, to], in_recv.at[n, me], (base + to, d),
            ).start()

    pltpu.make_async_copy(x_ref.at[:, col(d, 256)], x_all.at[d], x_recv.at[d]).start()

    @pl.loop(1, DPN)
    def _(i):
        to = (d + i) % DPN
        remote(x_ref.at[:, col(to, 256)], x_all.at[d], x_send.at[to], x_recv.at[d], (s, to)).start()

    w_copy = pltpu.make_async_copy(w_ref, w_all, w_sem)
    w_copy.start()

    for r in range(2):
        arrived(rlam.at[r], lam_recv.at[r])
    row = lax.broadcasted_iota(jnp.int32, (BLOCK, BLOCK), 0)
    column = lax.broadcasted_iota(jnp.int32, (BLOCK, BLOCK), 1)
    ones = jnp.ones((BLOCK, BLOCK), F32)
    hi = lax.Precision.HIGHEST

    @pl.loop(0, GROUP)
    def _(b):
        kept = []
        for r in range(2):
            lam = jnp.broadcast_to(rlam[r, pl.ds(b, 1), :], (BLOCK, BLOCK))
            seen = column <= row if r == 0 else column >= row
            c = dot(jnp.where(seen, lam, 0.0), ones, 1, 0, hi)
            kept.append(c - c.T)
            end = c[BLOCK - 1 : BLOCK, :] if r == 0 else c[0:1, :]
            qs[r, b] = jnp.exp(c) * 0.0625
            ks[r, b] = jnp.exp(end - c)
            ee[r, b] = jnp.broadcast_to(end, (8, 128))
        wgt[b] = jnp.exp(jnp.where(column <= row, kept[0], kept[1])) * 0.0625

    for r in range(2):
        up = jnp.zeros((8, 128), F32)
        down = jnp.zeros((8, 128), F32)
        for b in range(GROUP):
            tails[r, 1, b] = jnp.exp(down)
            down = down + ee[r, b]
            tails[r, 0, GROUP - 1 - b] = jnp.exp(up)
            up = up + ee[r, GROUP - 1 - b]
        for b in range(GROUP):
            ee[r, b] = jnp.exp(ee[r, b])

    m_st[...] = jnp.zeros_like(m_st)
    g_st[...] = jnp.zeros_like(g_st)

    @pl.loop(0, GROUP)
    def _(i):
        b = (me + GROUP - i) % GROUP
        for n, (_, dst, _) in enumerate(pairs):
            arrived(dst.at[b], in_recv.at[n, b])
        q, k, v, g = rq[b], rk[b], rv[b], rg[b]
        rm, rgr = gz, 1 - gz
        km = ks[rm, b] * tails[rm, gz, b][0:1, :]
        qg = qs[rgr, b] * tails[rgr, gz, b][0:1, :]
        m_st[...] += dot((k.astype(F32) * lanes(km, DK)).astype(BF16), v, 0, 0)
        g_st[...] += dot((q.astype(F32) * lanes(qg, DK)).astype(BF16), g, 0, 0)
        w = wgt[b]
        sc = (dot(q, k, 1, 1) * w).astype(BF16)
        gs = (dot(g, v, 1, 1) * w).astype(BF16)
        acc_v[b] = dot(sc, g, 0, 0)
        acc_q[b] = dot(gs, k, 1, 0)
        acc_k[b] = dot(gs, q, 0, 0)

    st_tx[0] = m_st[...].astype(BF16)
    st_tx[1] = g_st[...].astype(BF16)
    for n in range(2):
        remote(st_tx.at[n], st_rx.at[n], st_send.at[n], st_recv.at[n], (partner, d)).start()

    def step(b, way):
        rm, rgr = way, 1 - way
        q, k, v, g = rq[b], rk[b], rv[b], rg[b]
        kf = k.astype(F32)
        mb, gb = m_st[...].astype(BF16), g_st[...].astype(BF16)
        ksg = lanes(ks[rgr, b], DK)
        dq = dot(g, mb, 1, 1) * lanes(qs[rm, b], DK)
        dk = dot(v, gb, 1, 1) * ksg
        dv = dot((kf * ksg).astype(BF16), gb, 1, 0)
        kd = (kf * lanes(ks[rm, b], DK)).astype(BF16)
        qd = (q.astype(F32) * lanes(qs[rgr, b], DK)).astype(BF16)
        m_st[...] = m_st[...] * lanes(ee[rm, b][0:1, :], DV) + dot(kd, v, 0, 0)
        g_st[...] = g_st[...] * lanes(ee[rgr, b][0:1, :], DV) + dot(qd, g, 0, 0)
        return dq, dk, dv

    m_st[...] = jnp.zeros_like(m_st)
    g_st[...] = jnp.zeros_like(g_st)

    @pl.loop(0, GROUP)
    def _(i):
        b = i + gz * (GROUP - 1 - 2 * i)
        dq, dk, dv = step(b, gz)
        acc_q[b] += dq
        acc_k[b] += dk
        acc_v[b] += dv

    for n in range(2):
        arrived(st_rx.at[n], st_recv.at[n])
    m_st[...] = st_rx[0].astype(F32)
    g_st[...] = st_rx[1].astype(F32)

    homes = (
        (out_k, dk_all.at[d], DK),
        (out_q, dq_ref, DK),
        (out_v, dv_ref, DV),
    )

    def send_home(b, n):
        src, dst, width = homes[n]

        @pl.when(b == me)
        def _():
            pltpu.make_async_copy(src.at[b], dst.at[:, col(head, width)], out_recv.at[n, head]).start()

        @pl.when(b != me)
        def _():
            remote(
                src.at[b], dst.at[:, col(head, width)],
                out_send.at[n, b], out_recv.at[n, head], (base + b, d),
            ).start()

    @pl.loop(0, GROUP)
    def _(i):
        b = i + (1 - gz) * (GROUP - 1 - 2 * i)
        dq, dk, dv = step(b, 1 - gz)
        out_k[b] = (acc_k[b] + dk).astype(BF16)
        send_home(b, 0)
        out_q[b] = (acc_q[b] + dq).astype(BF16)
        out_v[b] = (acc_v[b] + dv).astype(BF16)

    @pl.loop(0, GROUP)
    def _(i):
        b = (me + i) % GROUP
        send_home(b, 1)
        send_home(b, 2)

    @pl.loop(0, GROUP)
    def _(h):
        arrived(out_k.at[h], out_recv.at[0, h])

    own = dk_all.at[d]
    remote(own, own, dk_send.at[sibling], dk_recv.at[d], (s, sibling)).start()
    for t in (1, 3, 2):
        to = 2 * ((xi + t) % 4) + core
        remote(own, own, dk_send.at[to], dk_recv.at[d], (s, to)).start()

    @pl.loop(0, DPN)
    def _(j):
        arrived(x_all.at[j], x_recv.at[j])

    w_copy.wait()
    dw_acc[...] = jnp.zeros_like(dw_acc)

    def take(j):
        dx_st[j] = dot(dk_all[j], w_all[...], 1, 1).astype(BF16)
        xt = x_all[j]

        @pl.loop(0, 4)
        def _(c):
            dw_acc[:, col(c, 512)] += dot(xt, dk_all[j, :, col(c, 512)], 0, 0)

    def give(j):
        remote(dx_st.at[j], dx_ref.at[:, col(d, 256)], dx_send.at[j], dx_recv.at[d], (s, j)).start()

    take(d)
    pltpu.make_async_copy(dx_st.at[d], dx_ref.at[:, col(d, 256)], dx_recv.at[d]).start()
    arrived(dk_all.at[sibling], dk_recv.at[sibling])
    take(sibling)
    give(sibling)

    @pl.loop(0, 3)
    def _(i):
        t = 1 + (2 * i) % 3
        near = 2 * ((xi + t) % 4) + core
        far = 2 * ((xi + t) % 4) + 1 - core
        arrived(dk_all.at[near], dk_recv.at[near])
        remote(dk_all.at[near], dk_all.at[near], dk_fwd.at[i], dk_recv.at[near], (s, sibling)).start()
        take(near)
        give(near)
        arrived(dk_all.at[far], dk_recv.at[far])
        take(far)
        give(far)

    for j in range(SP):
        dw_tx[j] = dw_acc[:, 128 * j : 128 * (j + 1)].astype(BF16)
    pltpu.make_async_copy(dw_tx.at[s], dw_rx.at[s], rs_recv.at[s]).start()

    @pl.loop(1, SP)
    def _(i):
        to = (s + i) % SP
        remote(dw_tx.at[to], dw_rx.at[s], rs_send.at[to], rs_recv.at[s], (to, d)).start()

    @pl.loop(0, SP)
    def _(j):
        arrived(dw_rx.at[j], rs_recv.at[j])

    total = dw_rx[0].astype(F32)
    for j in range(1, SP):
        total += dw_rx[j].astype(F32)
    sum_tx[...] = total.astype(BF16)
    pltpu.make_async_copy(sum_tx, sum_rx.at[s], ag_recv.at[s]).start()

    @pl.loop(1, SP)
    def _(i):
        to = (s + i) % SP
        remote(sum_tx, sum_rx.at[s], ag_send.at[to], ag_recv.at[s], (to, d)).start()

    @pl.loop(0, SP)
    def _(j):
        arrived(sum_rx.at[j], ag_recv.at[j])

    for j in range(SP):
        dw_ref[:, 128 * j : 128 * (j + 1)] = sum_rx[j].astype(F32)

    @pl.loop(0, GROUP)
    def _(h):
        arrived(out_q.at[h], out_recv.at[1, h])
        arrived(out_v.at[h], out_recv.at[2, h])

    @pl.loop(0, DPN)
    def _(j):
        arrived(dx_st.at[j], dx_recv.at[j])

    for half in range(2):

        @pl.when(lam_to[half] != s)
        def _():
            arrived(rlam.at[half], lam_send.at[half])

    @pl.loop(1, GROUP)
    def _(i):
        to = (me + i) % GROUP
        for n, (_, dst, _) in enumerate(pairs):
            arrived(dst.at[to], in_send.at[n, to])
        for n, (src, _, _) in enumerate(homes):
            arrived(src.at[to], out_send.at[n, to])

    @pl.loop(1, DPN)
    def _(i):
        to = (d + i) % DPN
        arrived(x_all.at[to], x_send.at[to])
        arrived(dx_st.at[to], dx_send.at[to])

    for n in range(2):
        arrived(st_tx.at[n], st_send.at[n])
    arrived(own, dk_send.at[sibling])
    for t in range(1, 4):
        arrived(own, dk_send.at[2 * ((xi + t) % 4) + core])
        arrived(own, dk_fwd.at[t - 1])

    @pl.loop(1, SP)
    def _(i):
        to = (s + i) % SP
        arrived(sum_tx, rs_send.at[to])
        arrived(sum_tx, ag_send.at[to])


def step(x, q, k, v, g, lam, w):
    vmem = pl.BlockSpec(memory_space=pltpu.VMEM)
    hbm = pl.BlockSpec(memory_space=pl.ANY)
    dma = pltpu.SemaphoreType.DMA
    v_ = pltpu.VMEM
    dq, dv, dx, dw = pl.pallas_call(
        kernel,
        out_shape=(
            jax.ShapeDtypeStruct((BLOCK, 2048), BF16),
            jax.ShapeDtypeStruct((BLOCK, 4096), BF16),
            jax.ShapeDtypeStruct((BLOCK, 2048), BF16),
            jax.ShapeDtypeStruct((256, 2048), F32),
        ),
        in_specs=[hbm, vmem, vmem, vmem, vmem, vmem, hbm],
        out_specs=(vmem,) * 4,
        scratch_shapes=[
            v_((8, BLOCK, DK), BF16), v_((8, BLOCK, DK), BF16),
            v_((8, BLOCK, DV), BF16), v_((8, BLOCK, DV), BF16),
            v_((2, 8, 128), F32), v_((256, 2048), BF16), v_((8, BLOCK, 256), BF16),
            v_((2, 8, BLOCK, 128), F32), v_((2, 8, BLOCK, 128), F32),
            v_((2, 8, 8, 128), F32), v_((2, 2, 8, 8, 128), F32), v_((8, BLOCK, 128), F32),
            v_((8, BLOCK, DK), F32), v_((8, BLOCK, DK), F32), v_((8, BLOCK, DV), F32),
            v_((DK, DV), F32), v_((DK, DV), F32), v_((2, DK, DV), BF16), v_((2, DK, DV), BF16),
            v_((8, BLOCK, DK), BF16), v_((8, BLOCK, DK), BF16), v_((8, BLOCK, DV), BF16),
            v_((8, BLOCK, 2048), BF16), v_((8, BLOCK, 256), BF16),
            v_((256, 2048), F32), v_((16, 256, 128), BF16), v_((16, 256, 128), BF16),
            v_((256, 128), BF16), v_((16, 256, 128), BF16),
            dma((4, 8)), dma((4, 8)), dma((2,)), dma((2,)), dma((8,)), dma((8,)), dma,
            dma((2,)), dma((2,)), dma((3, 8)), dma((3, 8)), dma((8,)), dma((3,)), dma((8,)),
            dma((8,)), dma((8,)), dma((16,)), dma((16,)), dma((16,)), dma((16,)),
        ],
        compiler_params=pltpu.CompilerParams(
            collective_id=0, has_side_effects=True, vmem_limit_bytes=60 * 1024 * 1024
        ),
    )(x[0], q[0], k[0], v[0], g[0], lam[0].reshape(16, 128), w)
    return dq[None], dv[None], dx[None], dw


def solution(mesh):
    tokens = P("dp", "sp", None)
    return jax.shard_map(
        step,
        mesh=mesh,
        in_specs=(tokens,) * 6 + (P("dp", None),),
        out_specs=(tokens, tokens, tokens, P("dp", None)),
        check_vma=False,
    )
```

profile of v0, /device:TPU:6, one launch (start us, length us, event | category | flops | bytes accessed | tf_op | source)
XLA Modules:
  0.0 162.6 jit_solution(13893973027095851016)
XLA Ops:
  0.6 155.5 %shard_map.102 = (bf16[128,2048]{1,0:T(8,128)(2,1)}, bf16[128,4096]{1,0:T(8,128)(2,1)}, bf16[128,2048]{1,0:T(8,128)(2,1)}, f32[256,2048]{1,0:T(8,128)}) custom-call(bf16[128,2048]{1,0:T(8,128)(2,1)} %bitcast.12, bf16[128,2048]{1,0:T(8,128)(2,1)} %bitcast.13, bf16[128,2048]{1,0:T(8,128)(2,1)} %bitcast.14, bf16[128,4096]{1,0:T(8,128)(2,1)} %bitcast.10, ...), custom_call_target="tpu_custom_call" | custom-call | tf_op jit(solution)/shard_map/pallas_call | solution.py:360
  156.1 0.0 copy-start.1
  156.1 0.0 copy-start
  156.1 2.0 %copy.15 = bf16[1,128,2048]{2,1,0:T(8,128)(2,1)} copy(bf16[1,128,2048]{2,1,0:T(8,128)(2,1)} %bitcast.16) | data formatting | bytes 1048576
  158.2 2.3 %copy.16 = bf16[1,128,4096]{2,1,0:T(8,128)(2,1)} copy(bf16[1,128,4096]{2,1,0:T(8,128)(2,1)} %bitcast.9) | data formatting | bytes 2097152
  160.4 0.0 copy-done.1
  160.4 0.8 copy.17
  161.2 0.0 copy-done
  161.2 1.3 copy.18
Async XLA Ops:
  156.1 4.3 %copy-start.1 = (bf16[128,2048]{1,0:T(8,128)(2,1)S(1)}, bf16[128,2048]{1,0:T(8,128)(2,1)}, u32[]{:S(2)}) copy-start(bf16[128,2048]{1,0:T(8,128)(2,1)} %get-tuple-element.10) | copy-start | bytes 1572868
  156.1 5.1 %copy-start = (f32[256,2048]{1,0:T(8,128)S(1)}, f32[256,2048]{1,0:T(8,128)}, u32[]{:S(2)}) copy-start(f32[256,2048]{1,0:T(8,128)} %get-tuple-element.19) | copy-start | bytes 6291460
where the time goes:
time: 163 us
  Pallas kernels  155 us (95%)
  local copies, waits for them, and re-layouts  6.44 us (4%)
    pallas_call x1, Pallas kernels, step(): pl.pallas_call(kernel, out_shape=(jax.ShapeDtypeStruct((BLOCK, 2048), BF1...  155 us
    unnamed x8, local copies, waits for them, and re-layouts  6.44 us

commit v1 on v0

v1 whole, which is shorter than its diff:
```python
import functools

import jax
import jax.numpy as jnp
from jax import lax
from jax.experimental import pallas as pl
from jax.experimental.pallas import tpu as pltpu
from jax.sharding import PartitionSpec as P

F32 = jnp.float32
BF16 = jnp.bfloat16
SP, DPN = 16, 8
GROUP = 8
DK, DV, D = 256, 512, 2048
BLOCK = 128
CHUNKS = 4
CHUNK = D // CHUNKS
MESH = pl.DeviceIdType.MESH


def dot(a, b, ca, cb, precision=None):
    return lax.dot_general(
        a, b, (((ca,), (cb,)), ((), ())), preferred_element_type=F32, precision=precision
    )


def lanes(scale, width):
    return jnp.concatenate([scale] * (width // 128), axis=1)


def kernel(
    x_ref, q_ref, k_ref, v_ref, g_ref, lam_ref, w_ref,
    dq_ref, dv_ref, dx_ref, dw_ref,
    rq, rk, rv, rg, rlam, w_all, x_all,
    qs, ks, ee, tails, wgt,
    acc_q, gs_all, g_all, st, st_tx, st_rx, out_q, out_k, out_v,
    dk_all, dx_st, dx_acc, xt, dw_tx, dw_rx, sum_tx,
    in_send, in_recv, lam_send, lam_recv, x_send, x_recv, w_sem,
    st_send, st_recv, out_send, out_recv, dk_send, dk_fwd, dk_recv,
    dx_send, dx_recv, rs_send, rs_recv, ag_send, ag_recv,
):
    s = lax.axis_index("sp")
    d = lax.axis_index("dp")
    gz = s // GROUP
    me = s % GROUP
    head = (me + 4 * gz) % GROUP
    base = GROUP * gz
    partner = GROUP * (1 - gz) + (head + 4 * (1 - gz)) % GROUP
    xi, core = d // 2, d % 2
    sibling = 2 * xi + 1 - core

    def col(i, width):
        return pl.ds(pl.multiple_of(i * width, width), width)

    def remote(src, dst, ssem, rsem, to):
        return pltpu.make_async_remote_copy(
            src_ref=src, dst_ref=dst, send_sem=ssem, recv_sem=rsem,
            device_id=to, device_id_type=MESH,
        )

    def arrived(dst, sem):
        pltpu.make_async_copy(dst, dst, sem).wait()

    barrier = pltpu.get_barrier_semaphore()

    @pl.loop(1, SP)
    def _(i):
        pl.semaphore_signal(barrier, inc=1, device_id=((s + i) % SP, d), device_id_type=MESH)

    @pl.loop(1, DPN)
    def _(i):
        pl.semaphore_signal(barrier, inc=1, device_id=(s, (d + i) % DPN), device_id_type=MESH)

    pl.semaphore_wait(barrier, SP + DPN - 2)

    lam_to = [s // 2, GROUP + (s // 2 + 4) % GROUP]
    for half in range(2):
        src = lam_ref.at[pl.ds(8 * half, 8), :]

        @pl.when(lam_to[half] == s)
        def _():
            pltpu.make_async_copy(src, rlam.at[s % 2], lam_recv.at[s % 2]).start()

        @pl.when(lam_to[half] != s)
        def _():
            remote(src, rlam.at[s % 2], lam_send.at[half], lam_recv.at[s % 2], (lam_to[half], d)).start()

    pairs = ((g_ref, rg, DV), (q_ref, rq, DK), (v_ref, rv, DV), (k_ref, rk, DK))
    for n, (src, dst, width) in enumerate(pairs):
        pltpu.make_async_copy(src.at[:, col(head, width)], dst.at[me], in_recv.at[n, me]).start()

    for n, (src, dst, width) in enumerate(pairs):

        @pl.loop(1, GROUP)
        def _(i):
            to = (me + i) % GROUP
            its_head = (to + 4 * gz) % GROUP
            remote(
                src.at[:, col(its_head, width)], dst.at[me],
                in_send.at[n, to], in_recv.at[n, me], (base + to, d),
            ).start()

    pltpu.make_async_copy(x_ref.at[:, col(d, 256)], x_all.at[d], x_recv.at[d]).start()

    @pl.loop(1, DPN)
    def _(i):
        to = (d + i) % DPN
        remote(x_ref.at[:, col(to, 256)], x_all.at[d], x_send.at[to], x_recv.at[d], (s, to)).start()

    w_copy = pltpu.make_async_copy(w_ref, w_all, w_sem)
    w_copy.start()

    for r in range(2):
        arrived(rlam.at[r], lam_recv.at[r])
    row = lax.broadcasted_iota(jnp.int32, (BLOCK, BLOCK), 0)
    column = lax.broadcasted_iota(jnp.int32, (BLOCK, BLOCK), 1)
    ones = jnp.ones((BLOCK, BLOCK), F32)
    hi = lax.Precision.HIGHEST

    @pl.loop(0, GROUP)
    def _(b):
        kept = []
        for r in range(2):
            lam = jnp.broadcast_to(rlam[r, pl.ds(b, 1), :], (BLOCK, BLOCK))
            seen = column <= row if r == 0 else column >= row
            c = dot(jnp.where(seen, lam, 0.0), ones, 1, 0, hi)
            kept.append(c - c.T)
            end = c[BLOCK - 1 : BLOCK, :] if r == 0 else c[0:1, :]
            qs[r, b] = jnp.exp(c) * 0.0625
            ks[r, b] = jnp.exp(end - c)
            ee[r, b] = jnp.broadcast_to(end, (8, 128))
        wgt[b] = jnp.exp(jnp.where(column <= row, kept[0], kept[1])) * 0.0625

    for r in range(2):
        up = jnp.zeros((8, 128), F32)
        down = jnp.zeros((8, 128), F32)
        for b in range(GROUP):
            tails[r, 1, b] = jnp.exp(down)
            down = down + ee[r, b]
            tails[r, 0, GROUP - 1 - b] = jnp.exp(up)
            up = up + ee[r, GROUP - 1 - b]
        for b in range(GROUP):
            ee[r, b] = jnp.exp(ee[r, b])

    def order(i, way):
        return i + way * (GROUP - 1 - 2 * i)

    def send_state(st, n):
        st_tx[n] = st[...].astype(BF16)
        remote(st_tx.at[n], st_rx.at[n], st_send.at[n], st_recv.at[n], (partner, d)).start()

    def scaled(block, scale):
        return (block.astype(F32) * lanes(scale, DK)).astype(BF16)

    st[...] = jnp.zeros_like(st)

    @pl.loop(0, GROUP)
    def _(i):
        b = (me + GROUP - i) % GROUP
        for n in (0, 1):
            arrived(pairs[n][1].at[b], in_recv.at[n, b])
        st[...] += dot(scaled(rq[b], qs[1 - gz, b] * tails[1 - gz, gz, b][0:1, :]), rg[b], 0, 0)

    send_state(st, 0)

    def g_chain(way):
        r = 1 - way

        @pl.loop(0, GROUP)
        def _(i):
            b = order(i, way)
            g_all[r, b] = st[...].astype(BF16)
            st[...] = st[...] * lanes(ee[r, b][0:1, :], DV) + dot(scaled(rq[b], qs[r, b]), rg[b], 0, 0)

    st[...] = jnp.zeros_like(st)
    g_chain(gz)
    arrived(st_rx.at[0], st_recv.at[0])
    st[...] = st_rx[0].astype(F32)
    g_chain(1 - gz)

    homes = (
        (out_k, dk_all.at[d], DK),
        (out_v, dv_ref, DV),
        (out_q, dq_ref, DK),
    )

    def send_home(b, n):
        src, dst, width = homes[n]

        @pl.when(b == me)
        def _():
            pltpu.make_async_copy(src.at[b], dst.at[:, col(head, width)], out_recv.at[n, head]).start()

        @pl.when(b != me)
        def _():
            remote(
                src.at[b], dst.at[:, col(head, width)],
                out_send.at[n, b], out_recv.at[n, head], (base + b, d),
            ).start()

    st[...] = jnp.zeros_like(st)

    @pl.loop(0, GROUP)
    def _(i):
        b = (me + GROUP - i) % GROUP
        for n in (2, 3):
            arrived(pairs[n][1].at[b], in_recv.at[n, b])
        v = rv[b]
        gs = (dot(rg[b], v, 1, 1) * wgt[b]).astype(BF16)
        gs_all[b] = gs
        dk = dot(gs, rq[b], 0, 0)
        for r in range(2):
            dk += dot(v, g_all[r, b], 1, 1) * lanes(ks[r, b], DK)
        out_k[b] = dk.astype(BF16)
        send_home(b, 0)
        st[...] += dot(scaled(rk[b], ks[gz, b] * tails[gz, gz, b][0:1, :]), v, 0, 0)

    send_state(st, 1)

    @pl.loop(0, GROUP)
    def _(i):
        b = (me + GROUP - i) % GROUP
        k = rk[b]
        dv = dot((dot(rq[b], k, 1, 1) * wgt[b]).astype(BF16), rg[b], 0, 0)
        for r in range(2):
            dv += dot(scaled(k, ks[r, b]), g_all[r, b], 1, 0)
        out_v[b] = dv.astype(BF16)
        send_home(b, 1)

    def m_step(b, r):
        dq = dot(rg[b], st[...].astype(BF16), 1, 1) * lanes(qs[r, b], DK)
        st[...] = st[...] * lanes(ee[r, b][0:1, :], DV) + dot(scaled(rk[b], ks[r, b]), rv[b], 0, 0)
        return dq

    st[...] = jnp.zeros_like(st)

    @pl.loop(0, GROUP)
    def _(i):
        b = order(i, gz)
        acc_q[b] = m_step(b, gz) + dot(gs_all[b], rk[b], 1, 0)

    @pl.loop(0, GROUP)
    def _(h):
        arrived(out_k.at[h], out_recv.at[0, h])

    def piece(j, c):
        return dk_all.at[j, :, col(c, CHUNK)]

    for c in range(CHUNKS):
        own = piece(d, c)
        remote(own, own, dk_send.at[0, c], dk_recv.at[d, c], (s, sibling)).start()
        for t in (1, 3, 2):
            remote(own, own, dk_send.at[t, c], dk_recv.at[d, c], (s, 2 * ((xi + t) % 4) + core)).start()

    arrived(st_rx.at[1], st_recv.at[1])
    st[...] = st_rx[1].astype(F32)

    @pl.loop(0, GROUP)
    def _(i):
        b = order(i, 1 - gz)
        out_q[b] = (acc_q[b] + m_step(b, 1 - gz)).astype(BF16)
        send_home(b, 2)

    @pl.loop(0, DPN)
    def _(j):
        arrived(x_all.at[j], x_recv.at[j])
        xt[:, col(j, BLOCK)] = x_all[j].T

    w_copy.wait()
    dx_acc[...] = jnp.zeros_like(dx_acc)

    def sum_chunk(c):
        arrived(dw_rx.at[c], rs_recv.at[c])
        sum_tx[c] = jnp.sum(dw_rx[c].astype(F32), axis=0).astype(BF16)
        place = dw_ref.at[pl.ds(pl.multiple_of(16 * s, 16), 16), col(c, CHUNK)]
        pltpu.make_async_copy(sum_tx.at[c], place, ag_recv.at[c]).start()

        @pl.loop(1, SP)
        def _(i):
            remote(sum_tx.at[c], place, ag_send.at[c], ag_recv.at[c], ((s + i) % SP, d)).start()

    @pl.loop(0, CHUNKS)
    def _(c):
        arrived(piece(sibling, c), dk_recv.at[sibling, c])
        for n, t in enumerate((1, 3, 2)):
            near = 2 * ((xi + t) % 4) + core
            arrived(piece(near, c), dk_recv.at[near, c])
            remote(piece(near, c), piece(near, c), dk_fwd.at[n, c], dk_recv.at[near, c], (s, sibling)).start()
        for t in (1, 3, 2):
            far = 2 * ((xi + t) % 4) + 1 - core
            arrived(piece(far, c), dk_recv.at[far, c])
        part = dk_all[:, :, col(c, CHUNK)].reshape(DPN * BLOCK, CHUNK)
        dw_tx[c] = dot(xt[...], part, 1, 0).astype(BF16)
        pltpu.make_async_copy(
            dw_tx.at[c, pl.ds(pl.multiple_of(16 * s, 16), 16), :], dw_rx.at[c, s], rs_recv.at[c]
        ).start()

        @pl.loop(1, SP)
        def _(i):
            to = (s + i) % SP
            remote(
                dw_tx.at[c, pl.ds(pl.multiple_of(16 * to, 16), 16), :], dw_rx.at[c, s],
                rs_send.at[c], rs_recv.at[c], (to, d),
            ).start()

        dx_acc[...] += dot(part, w_all[:, col(c, CHUNK)], 1, 1)

        @pl.when(c > 0)
        def _():
            sum_chunk(c - 1)

    for j in range(DPN):
        dx_st[j] = dx_acc[BLOCK * j : BLOCK * (j + 1), :].astype(BF16)
    columns = dx_ref.at[:, col(d, 256)]
    pltpu.make_async_copy(dx_st.at[d], columns, dx_recv.at[d]).start()

    @pl.loop(1, DPN)
    def _(i):
        to = (d + i) % DPN
        remote(dx_st.at[to], columns, dx_send.at[to], dx_recv.at[d], (s, to)).start()

    sum_chunk(CHUNKS - 1)

    @pl.loop(0, GROUP)
    def _(h):
        arrived(out_v.at[h], out_recv.at[1, h])
        arrived(out_q.at[h], out_recv.at[2, h])

    @pl.loop(0, DPN)
    def _(j):
        arrived(dx_st.at[j], dx_recv.at[j])

    for half in range(2):

        @pl.when(lam_to[half] != s)
        def _():
            arrived(rlam.at[half], lam_send.at[half])

    @pl.loop(1, GROUP)
    def _(i):
        to = (me + i) % GROUP
        for n, (_, dst, _) in enumerate(pairs):
            arrived(dst.at[to], in_send.at[n, to])
        for n, (src, _, _) in enumerate(homes):
            arrived(src.at[to], out_send.at[n, to])

    @pl.loop(1, DPN)
    def _(i):
        to = (d + i) % DPN
        arrived(x_all.at[to], x_send.at[to])
        arrived(dx_st.at[to], dx_send.at[to])

    for n in range(2):
        arrived(st_tx.at[n], st_send.at[n])

    @pl.loop(0, CHUNKS)
    def _(c):
        own = piece(d, c)
        for t in range(4):
            arrived(own, dk_send.at[t, c])
        for t in range(3):
            arrived(own, dk_fwd.at[t, c])
        most = dw_rx.at[c, pl.ds(0, SP - 1)]
        arrived(most, rs_send.at[c])
        arrived(most, ag_send.at[c])
        arrived(dw_ref.at[:, col(c, CHUNK)], ag_recv.at[c])


def step(x, q, k, v, g, lam, w):
    vmem = pl.BlockSpec(memory_space=pltpu.VMEM)
    hbm = pl.BlockSpec(memory_space=pl.ANY)
    dma = pltpu.SemaphoreType.DMA
    v_ = pltpu.VMEM
    dq, dv, dx, dw = pl.pallas_call(
        kernel,
        out_shape=(
            jax.ShapeDtypeStruct((BLOCK, 2048), BF16),
            jax.ShapeDtypeStruct((BLOCK, 4096), BF16),
            jax.ShapeDtypeStruct((BLOCK, 2048), BF16),
            jax.ShapeDtypeStruct((256, 2048), BF16),
        ),
        in_specs=[hbm, vmem, vmem, vmem, vmem, vmem, hbm],
        out_specs=(vmem,) * 4,
        scratch_shapes=[
            v_((8, BLOCK, DK), BF16), v_((8, BLOCK, DK), BF16),
            v_((8, BLOCK, DV), BF16), v_((8, BLOCK, DV), BF16),
            v_((2, 8, 128), F32), v_((256, 2048), BF16), v_((8, BLOCK, 256), BF16),
            v_((2, 8, BLOCK, 128), F32), v_((2, 8, BLOCK, 128), F32),
            v_((2, 8, 8, 128), F32), v_((2, 2, 8, 8, 128), F32), v_((8, BLOCK, 128), F32),
            v_((8, BLOCK, DK), F32), v_((8, BLOCK, BLOCK), BF16), v_((2, 8, DK, DV), BF16),
            v_((DK, DV), F32), v_((2, DK, DV), BF16), v_((2, DK, DV), BF16),
            v_((8, BLOCK, DK), BF16), v_((8, BLOCK, DK), BF16), v_((8, BLOCK, DV), BF16),
            v_((8, BLOCK, D), BF16), v_((8, BLOCK, 256), BF16), v_((8 * BLOCK, 256), F32),
            v_((256, 8 * BLOCK), BF16), v_((CHUNKS, 256, CHUNK), BF16),
            v_((CHUNKS, 16, 16, CHUNK), BF16), v_((CHUNKS, 16, CHUNK), BF16),
            dma((4, 8)), dma((4, 8)), dma((2,)), dma((2,)), dma((8,)), dma((8,)), dma,
            dma((2,)), dma((2,)), dma((3, 8)), dma((3, 8)),
            dma((4, CHUNKS)), dma((3, CHUNKS)), dma((8, CHUNKS)), dma((8,)), dma((8,)),
            dma((CHUNKS,)), dma((CHUNKS,)), dma((CHUNKS,)), dma((CHUNKS,)),
        ],
        compiler_params=pltpu.CompilerParams(
            collective_id=0, has_side_effects=True, vmem_limit_bytes=60 * 1024 * 1024
        ),
    )(x[0], q[0], k[0], v[0], g[0], lam[0].reshape(16, 128), w)
    return dq[None], dv[None], dx[None], dw.astype(F32)


def solution(mesh):
    tokens = P("dp", "sp", None)
    return jax.shard_map(
        step,
        mesh=mesh,
        in_specs=(tokens,) * 6 + (P("dp", None),),
        out_specs=(tokens, tokens, tokens, P("dp", None)),
        check_vma=False,
    )
```

time: 163 us -> 111 us (0.68)
  the two profiles are of different devices: /device:TPU:6 before, /device:TPU:1 now
where the time goes in v1:
time: 111 us
  Pallas kernels  104 us (94%)
  other arithmetic  2.91 us (3%)
  local copies, waits for them, and re-layouts  2.57 us (2%)
    pallas_call x1, Pallas kernels, step(): pl.pallas_call(kernel, out_shape=(jax.ShapeDtypeStruct((BLOCK, 2048), BF1...  104 us
    convert_element_type x1, other arithmetic, step(): return (dq[None], dv[None], dx[None], dw.astype(F32))  2.91 us
    unnamed x9, local copies, waits for them, and re-layouts  2.57 us

profile of v1, /device:TPU:1, one launch (start us, length us, event | category | flops | bytes accessed | tf_op | source)
XLA Modules:
  0.0 110.6 jit_solution(4195447219648379988)
XLA Ops:
  0.6 104.5 %shard_map.102 = (bf16[128,2048]{1,0:T(8,128)(2,1)}, bf16[128,4096]{1,0:T(8,128)(2,1)}, bf16[128,2048]{1,0:T(8,128)(2,1)}, bf16[256,2048]{1,0:T(8,128)(2,1)}) custom-call(bf16[128,2048]{1,0:T(8,128)(2,1)} %bitcast.12, bf16[128,2048]{1,0:T(8,128)(2,1)} %bitcast.13, bf16[128,2048]{1,0:T(8,128)(2,1)} %bitcast.14, bf16[128,4096]{1,0:T(8,128)(2,1)} %bitcast.10, ...), custom_call_target="tpu_custom_call" | custom-call | tf_op jit(solution)/shard_map/pallas_call | solution.py:374
  105.1 0.0 copy-start.2
  105.1 0.0 copy-start
  105.1 2.9 %convert_element_type.3 = f32[256,2048]{1,0:T(8,128)} convert(bf16[256,2048]{1,0:T(8,128)(2,1)} %get-tuple-element.11) | non-fusion elementwise | flops 524288 | bytes 3145728 | tf_op jit(solution)/shard_map/convert_element_type | solution.py:405
  108.0 0.0 copy-done.2
  108.0 0.0 copy-start.1
  108.0 0.8 copy.14
  108.8 0.0 copy-done
  108.8 1.0 copy.15
  109.8 0.0 copy-done.1
  109.8 0.8 copy.16
Async XLA Ops:
  105.1 2.9 %copy-start.2 = (bf16[128,2048]{1,0:T(8,128)(2,1)S(1)}, bf16[128,2048]{1,0:T(8,128)(2,1)}, u32[]{:S(2)}) copy-start(bf16[128,2048]{1,0:T(8,128)(2,1)} %get-tuple-element.8) | copy-start | bytes 1572868
  105.1 3.7 %copy-start = (bf16[128,4096]{1,0:T(8,128)(2,1)S(1)}, bf16[128,4096]{1,0:T(8,128)(2,1)}, u32[]{:S(2)}) copy-start(bf16[128,4096]{1,0:T(8,128)(2,1)} %get-tuple-element.9) | copy-start | bytes 3145732
  108.0 1.8 %copy-start.1 = (bf16[128,2048]{1,0:T(8,128)(2,1)S(1)}, bf16[128,2048]{1,0:T(8,128)(2,1)}, u32[]{:S(2)}) copy-start(bf16[128,2048]{1,0:T(8,128)(2,1)} %get-tuple-element.10) | copy-start | bytes 1572868

commit v2 on v1

--- a/solution.py
+++ b/solution.py
@@ -34,7 +34,7 @@
     rq, rk, rv, rg, rlam, w_all, x_all,
     qs, ks, ee, tails, wgt,
     acc_q, gs_all, g_all, st, st_tx, st_rx, out_q, out_k, out_v,
-    dk_all, dx_st, dx_acc, xt, dw_tx, dw_rx, sum_tx,
+    dk_all, dx_st, dx_acc, xt, dw_tx, dw_rx, sum_tx, dw_sum,
     in_send, in_recv, lam_send, lam_recv, x_send, x_recv, w_sem,
     st_send, st_recv, out_send, out_recv, dk_send, dk_fwd, dk_recv,
     dx_send, dx_recv, rs_send, rs_recv, ag_send, ag_recv,
@@ -89,6 +89,8 @@
     for n, (src, dst, width) in enumerate(pairs):
         pltpu.make_async_copy(src.at[:, col(head, width)], dst.at[me], in_recv.at[n, me]).start()
 
+    pltpu.make_async_copy(x_ref.at[:, col(d, 256)], x_all.at[d], x_recv.at[d]).start()
+
     for n, (src, dst, width) in enumerate(pairs):
 
         @pl.loop(1, GROUP)
@@ -99,13 +101,9 @@
                 src.at[:, col(its_head, width)], dst.at[me],
                 in_send.at[n, to], in_recv.at[n, me], (base + to, d),
             ).start()
-
-    pltpu.make_async_copy(x_ref.at[:, col(d, 256)], x_all.at[d], x_recv.at[d]).start()
-
-    @pl.loop(1, DPN)
-    def _(i):
-        to = (d + i) % DPN
-        remote(x_ref.at[:, col(to, 256)], x_all.at[d], x_send.at[to], x_recv.at[d], (s, to)).start()
+            if n == 1:
+                its = (d + i) % DPN
+                remote(x_ref.at[:, col(its, 256)], x_all.at[d], x_send.at[its], x_recv.at[d], (s, its)).start()
 
     w_copy = pltpu.make_async_copy(w_ref, w_all, w_sem)
     w_copy.start()
@@ -198,13 +196,10 @@
                 out_send.at[n, b], out_recv.at[n, head], (base + b, d),
             ).start()
 
-    st[...] = jnp.zeros_like(st)
-
     @pl.loop(0, GROUP)
     def _(i):
         b = (me + GROUP - i) % GROUP
-        for n in (2, 3):
-            arrived(pairs[n][1].at[b], in_recv.at[n, b])
+        arrived(rv.at[b], in_recv.at[2, b])
         v = rv[b]
         gs = (dot(rg[b], v, 1, 1) * wgt[b]).astype(BF16)
         gs_all[b] = gs
@@ -213,9 +208,26 @@
             dk += dot(v, g_all[r, b], 1, 1) * lanes(ks[r, b], DK)
         out_k[b] = dk.astype(BF16)
         send_home(b, 0)
-        st[...] += dot(scaled(rk[b], ks[gz, b] * tails[gz, gz, b][0:1, :]), v, 0, 0)
+
+    st[...] = jnp.zeros_like(st)
+
+    @pl.loop(0, GROUP)
+    def _(i):
+        b = (me + GROUP - i) % GROUP
+        arrived(rk.at[b], in_recv.at[3, b])
+        st[...] += dot(scaled(rk[b], ks[gz, b] * tails[gz, gz, b][0:1, :]), rv[b], 0, 0)
 
     send_state(st, 1)
+
+    def piece(j, c):
+        return dk_all.at[j, :, col(c, CHUNK)]
+
+    left = 2 * ((xi + 3) % 4) + core
+    right = 2 * ((xi + 1) % 4) + core
+    across = 2 * ((xi + 2) % 4) + core
+
+    def pass_on(j, c, sem, to):
+        remote(piece(j, c), piece(j, c), sem, dk_recv.at[j, c], (s, to)).start()
 
     @pl.loop(0, GROUP)
     def _(i):
@@ -227,6 +239,20 @@
         out_v[b] = dv.astype(BF16)
         send_home(b, 1)
 
+        c = i // 2
+
+        @pl.when(i % 2 == 0)
+        def _():
+            for h in range(CHUNK // DK):
+                arrived(out_k.at[0], out_recv.at[0, c * (CHUNK // DK) + h])
+            pass_on(d, c, dk_send.at[0, c], left)
+            pass_on(d, c, dk_send.at[1, c], right)
+
+        @pl.when(i % 2 == 1)
+        def _():
+            pass_on(d, c, dk_send.at[2, c], across)
+            pass_on(d, c, dk_send.at[3, c], sibling)
+
     def m_step(b, r):
         dq = dot(rg[b], st[...].astype(BF16), 1, 1) * lanes(qs[r, b], DK)
         st[...] = st[...] * lanes(ee[r, b][0:1, :], DV) + dot(scaled(rk[b], ks[r, b]), rv[b], 0, 0)
@@ -239,28 +265,6 @@
         b = order(i, gz)
         acc_q[b] = m_step(b, gz) + dot(gs_all[b], rk[b], 1, 0)
 
-    @pl.loop(0, GROUP)
-    def _(h):
-        arrived(out_k.at[h], out_recv.at[0, h])
-
-    def piece(j, c):
-        return dk_all.at[j, :, col(c, CHUNK)]
-
-    for c in range(CHUNKS):
-        own = piece(d, c)
-        remote(own, own, dk_send.at[0, c], dk_recv.at[d, c], (s, sibling)).start()
-        for t in (1, 3, 2):
-            remote(own, own, dk_send.at[t, c], dk_recv.at[d, c], (s, 2 * ((xi + t) % 4) + core)).start()
-
-    arrived(st_rx.at[1], st_recv.at[1])
-    st[...] = st_rx[1].astype(F32)
-
-    @pl.loop(0, GROUP)
-    def _(i):
-        b = order(i, 1 - gz)
-        out_q[b] = (acc_q[b] + m_step(b, 1 - gz)).astype(BF16)
-        send_home(b, 2)
-
     @pl.loop(0, DPN)
     def _(j):
         arrived(x_all.at[j], x_recv.at[j])
@@ -269,10 +273,19 @@
     w_copy.wait()
     dx_acc[...] = jnp.zeros_like(dx_acc)
 
+    arrived(st_rx.at[1], st_recv.at[1])
+    st[...] = st_rx[1].astype(F32)
+
+    @pl.loop(0, GROUP)
+    def _(i):
+        b = order(i, 1 - gz)
+        out_q[b] = (acc_q[b] + m_step(b, 1 - gz)).astype(BF16)
+        send_home(b, 2)
+
     def sum_chunk(c):
         arrived(dw_rx.at[c], rs_recv.at[c])
         sum_tx[c] = jnp.sum(dw_rx[c].astype(F32), axis=0).astype(BF16)
-        place = dw_ref.at[pl.ds(pl.multiple_of(16 * s, 16), 16), col(c, CHUNK)]
+        place = dw_sum.at[pl.ds(pl.multiple_of(16 * s, 16), 16), col(c, CHUNK)]
         pltpu.make_async_copy(sum_tx.at[c], place, ag_recv.at[c]).start()
 
         @pl.loop(1, SP)
@@ -281,13 +294,11 @@
 
     @pl.loop(0, CHUNKS)
     def _(c):
-        arrived(piece(sibling, c), dk_recv.at[sibling, c])
-        for n, t in enumerate((1, 3, 2)):
-            near = 2 * ((xi + t) % 4) + core
-            arrived(piece(near, c), dk_recv.at[near, c])
-            remote(piece(near, c), piece(near, c), dk_fwd.at[n, c], dk_recv.at[near, c], (s, sibling)).start()
-        for t in (1, 3, 2):
-            far = 2 * ((xi + t) % 4) + 1 - core
+        for n, j in enumerate((left, right, across)):
+            arrived(piece(j, c), dk_recv.at[j, c])
+            pass_on(j, c, dk_fwd.at[n, c], sibling)
+        for j in range(4):
+            far = 2 * ((xi + j) % 4) + 1 - core
             arrived(piece(far, c), dk_recv.at[far, c])
         part = dk_all[:, :, col(c, CHUNK)].reshape(DPN * BLOCK, CHUNK)
         dw_tx[c] = dot(xt[...], part, 1, 0).astype(BF16)
@@ -363,7 +374,17 @@
         most = dw_rx.at[c, pl.ds(0, SP - 1)]
         arrived(most, rs_send.at[c])
         arrived(most, ag_send.at[c])
-        arrived(dw_ref.at[:, col(c, CHUNK)], ag_recv.at[c])
+        arrived(dw_sum.at[:, col(c, CHUNK)], ag_recv.at[c])
+        dw_ref[:, col(c, CHUNK)] = dw_sum[:, col(c, CHUNK)].astype(F32)
+
+
+def write_out(*refs):
+    sems = refs[-1]
+    copies = [pltpu.make_async_copy(refs[n], refs[n + 4], sems.at[n]) for n in range(4)]
+    for copy in copies:
+        copy.start()
+    for copy in copies:
+        copy.wait()
 
 
 def step(x, q, k, v, g, lam, w):
@@ -371,15 +392,12 @@
     hbm = pl.BlockSpec(memory_space=pl.ANY)
     dma = pltpu.SemaphoreType.DMA
     v_ = pltpu.VMEM
-    dq, dv, dx, dw = pl.pallas_call(
+    results = pl.pallas_call(
         kernel,
         out_shape=(
-            jax.ShapeDtypeStruct((BLOCK, 2048), BF16),
-            jax.ShapeDtypeStruct((BLOCK, 4096), BF16),
-            jax.ShapeDtypeStruct((BLOCK, 2048), BF16),
-            jax.ShapeDtypeStruct((256, 2048), BF16),
+            v_((BLOCK, 2048), BF16), v_((BLOCK, 4096), BF16), v_((BLOCK, 2048), BF16), v_((256, 2048), F32)
         ),
-        in_specs=[hbm, vmem, vmem, vmem, vmem, vmem, hbm],
+        in_specs=[hbm, hbm, hbm, hbm, hbm, vmem, hbm],
         out_specs=(vmem,) * 4,
         scratch_shapes=[
             v_((8, BLOCK, DK), BF16), v_((8, BLOCK, DK), BF16),
@@ -392,17 +410,25 @@
             v_((8, BLOCK, DK), BF16), v_((8, BLOCK, DK), BF16), v_((8, BLOCK, DV), BF16),
             v_((8, BLOCK, D), BF16), v_((8, BLOCK, 256), BF16), v_((8 * BLOCK, 256), F32),
             v_((256, 8 * BLOCK), BF16), v_((CHUNKS, 256, CHUNK), BF16),
-            v_((CHUNKS, 16, 16, CHUNK), BF16), v_((CHUNKS, 16, CHUNK), BF16),
+            v_((CHUNKS, 16, 16, CHUNK), BF16), v_((CHUNKS, 16, CHUNK), BF16), v_((256, D), BF16),
             dma((4, 8)), dma((4, 8)), dma((2,)), dma((2,)), dma((8,)), dma((8,)), dma,
             dma((2,)), dma((2,)), dma((3, 8)), dma((3, 8)),
             dma((4, CHUNKS)), dma((3, CHUNKS)), dma((8, CHUNKS)), dma((8,)), dma((8,)),
             dma((CHUNKS,)), dma((CHUNKS,)), dma((CHUNKS,)), dma((CHUNKS,)),
         ],
         compiler_params=pltpu.CompilerParams(
-            collective_id=0, has_side_effects=True, vmem_limit_bytes=60 * 1024 * 1024
+            collective_id=0, has_side_effects=True, vmem_limit_bytes=58 * 1024 * 1024
         ),
     )(x[0], q[0], k[0], v[0], g[0], lam[0].reshape(16, 128), w)
-    return dq[None], dv[None], dx[None], dw.astype(F32)
+    dq, dv, dx, dw = pl.pallas_call(
+        write_out,
+        out_shape=tuple(pltpu.HBM(a.shape, a.dtype) for a in results),
+        in_specs=[hbm] * 4,
+        out_specs=(hbm,) * 4,
+        scratch_shapes=[dma((4,))],
+        compiler_params=pltpu.CompilerParams(vmem_limit_bytes=20 * 1024 * 1024),
+    )(*results)
+    return dq[None], dv[None], dx[None], dw
 
 
 def solution(mesh):

time: 111 us -> 105 us (0.946)
  other arithmetic: 2.91 us -> 0 us
  local copies, waits for them, and re-layouts: 2.57 us -> 0 us
    convert_element_type x1 -> x0, other arithmetic: 2.91 us -> none  [step(): return (dq[None], dv[None], dx[None], dw.astype(F32))]
    unnamed x9 -> x0, local copies, waits for them, and re-layouts: 2.57 us -> none
    pallas_call x1 -> x2, Pallas kernels: 104 us -> 104 us  [the longest x1 101 us: step(): pl.pallas_call(kernel, out_shape=(v_((BLOCK, 2048), BF16), v_((BLOCK, 409...]
where the time goes in v2:
time: 105 us; the launch traced here: 104 us
  Pallas kernels  104 us (99%)
    pallas_call x1, Pallas kernels, step(): pl.pallas_call(kernel, out_shape=(v_((BLOCK, 2048), BF16), v_((BLOCK, 409...  101 us

profile of v2, /device:TPU:1, one launch (start us, length us, event | category | flops | bytes accessed | tf_op | source)
XLA Modules:
  0.0 104.2 jit_solution(9552770239942843878)
XLA Ops:
  0.6 101.5 %shard_map.102 = (bf16[128,2048]{1,0:T(8,128)(2,1)S(1)}, bf16[128,4096]{1,0:T(8,128)(2,1)S(1)}, bf16[128,2048]{1,0:T(8,128)(2,1)S(1)}, f32[256,2048]{1,0:T(8,128)S(1)}) custom-call(bf16[128,2048]{1,0:T(8,128)(2,1)} %bitcast.11, bf16[128,2048]{1,0:T(8,128)(2,1)} %bitcast.12, bf16[128,2048]{1,0:T(8,128)(2,1)} %bitcast.13, bf16[128,4096]{1,0:T(8,128)(2,1)} %bitcast.9, ...), custom_call_target="tpu_custom_call" | custom-call | tf_op jit(solution)/shard_map/pallas_call | solution.py:395
  102.1 2.0 %shard_map.103 = (bf16[128,2048]{1,0:T(8,128)(2,1)}, bf16[128,4096]{1,0:T(8,128)(2,1)}, bf16[128,2048]{1,0:T(8,128)(2,1)}, f32[256,2048]{1,0:T(8,128)}) custom-call(bf16[128,2048]{1,0:T(8,128)(2,1)S(1)} %get-tuple-element.12.refs_0_, bf16[128,4096]{1,0:T(8,128)(2,1)S(1)} %get-tuple-element.13.refs_1_, bf16[128,2048]{1,0:T(8,128)(2,1)S(1)} %get-tuple-element.14.refs_2_, ...), custom_call_target="tpu_custom_call" | custom-call | tf_op jit(solution)/shard_map/pallas_call | solution.py:423

commit v3 on v2

--- a/solution.py
+++ b/solution.py
@@ -15,6 +15,7 @@
 BLOCK = 128
 CHUNKS = 4
 CHUNK = D // CHUNKS
+LAST = CHUNKS - 1
 MESH = pl.DeviceIdType.MESH
 
 
@@ -34,10 +35,10 @@
     rq, rk, rv, rg, rlam, w_all, x_all,
     qs, ks, ee, tails, wgt,
     acc_q, gs_all, g_all, st, st_tx, st_rx, out_q, out_k, out_v,
-    dk_all, dx_st, dx_acc, xt, dw_tx, dw_rx, sum_tx, dw_sum,
+    dk_all, dx_st, dx_acc, xt, dw_tx, rx_one, tx_two, rx_two, dw_rx, sum_tx, dw_sum,
     in_send, in_recv, lam_send, lam_recv, x_send, x_recv, w_sem,
     st_send, st_recv, out_send, out_recv, dk_send, dk_fwd, dk_recv,
-    dx_send, dx_recv, rs_send, rs_recv, ag_send, ag_recv,
+    dx_send, dx_recv, sum_send, sum_recv, last_send, last_recv,
 ):
     s = lax.axis_index("sp")
     d = lax.axis_index("dp")
@@ -89,13 +90,23 @@
     for n, (src, dst, width) in enumerate(pairs):
         pltpu.make_async_copy(src.at[:, col(head, width)], dst.at[me], in_recv.at[n, me]).start()
 
+    row_here, y_here = me // 4, me % 4
+    near_y = (y_here + 1 - 2 * (y_here % 2), 3 - y_here)
+    farthest_first = [4 * (1 - row_here) + (y_here + 2) % 4, 4 * row_here + (y_here + 2) % 4]
+    farthest_first += [4 * (1 - row_here) + y for y in near_y] + [4 * (1 - row_here) + y_here]
+    farthest_first += [4 * row_here + y for y in near_y]
+
+    def nth(i):
+        b = me
+        for n, to in enumerate(farthest_first):
+            b = jnp.where(i == n, to, b)
+        return b
+
     pltpu.make_async_copy(x_ref.at[:, col(d, 256)], x_all.at[d], x_recv.at[d]).start()
 
     for n, (src, dst, width) in enumerate(pairs):
 
-        @pl.loop(1, GROUP)
-        def _(i):
-            to = (me + i) % GROUP
+        for i, to in enumerate(farthest_first, 1):
             its_head = (to + 4 * gz) % GROUP
             remote(
                 src.at[:, col(its_head, width)], dst.at[me],
@@ -154,7 +165,7 @@
 
     @pl.loop(0, GROUP)
     def _(i):
-        b = (me + GROUP - i) % GROUP
+        b = nth(i)
         for n in (0, 1):
             arrived(pairs[n][1].at[b], in_recv.at[n, b])
         st[...] += dot(scaled(rq[b], qs[1 - gz, b] * tails[1 - gz, gz, b][0:1, :]), rg[b], 0, 0)
@@ -198,7 +209,7 @@
 
     @pl.loop(0, GROUP)
     def _(i):
-        b = (me + GROUP - i) % GROUP
+        b = nth(i)
         arrived(rv.at[b], in_recv.at[2, b])
         v = rv[b]
         gs = (dot(rg[b], v, 1, 1) * wgt[b]).astype(BF16)
@@ -213,7 +224,7 @@
 
     @pl.loop(0, GROUP)
     def _(i):
-        b = (me + GROUP - i) % GROUP
+        b = nth(i)
         arrived(rk.at[b], in_recv.at[3, b])
         st[...] += dot(scaled(rk[b], ks[gz, b] * tails[gz, gz, b][0:1, :]), rv[b], 0, 0)
 
@@ -231,7 +242,7 @@
 
     @pl.loop(0, GROUP)
     def _(i):
-        b = (me + GROUP - i) % GROUP
+        b = nth(i)
         k = rk[b]
         dv = dot((dot(rq[b], k, 1, 1) * wgt[b]).astype(BF16), rg[b], 0, 0)
         for r in range(2):
@@ -280,20 +291,101 @@
     def _(i):
         b = order(i, 1 - gz)
         out_q[b] = (acc_q[b] + m_step(b, 1 - gz)).astype(BF16)
-        send_home(b, 2)
-
-    def sum_chunk(c):
-        arrived(dw_rx.at[c], rs_recv.at[c])
-        sum_tx[c] = jnp.sum(dw_rx[c].astype(F32), axis=0).astype(BF16)
-        place = dw_sum.at[pl.ds(pl.multiple_of(16 * s, 16), 16), col(c, CHUNK)]
-        pltpu.make_async_copy(sum_tx.at[c], place, ag_recv.at[c]).start()
+
+    @pl.loop(0, GROUP)
+    def _(i):
+        send_home(nth(i), 2)
+
+    sz, sy = s // 4, s % 4
+
+    def axes(c):
+        odd = c % 2
+        one, two = sz + odd * (sy - sz), sy + odd * (sz - sy)
+
+        def device(i, j):
+            return (4 * i + j + odd * (3 * j - 3 * i), d)
+
+        return one, two, device
+
+    def rows(i, n):
+        return pl.ds(pl.multiple_of(i * n, n), n)
+
+    def first_sums(c):
+        one, two, device = axes(c)
+        pltpu.make_async_copy(dw_tx.at[c, rows(one, 64)], rx_one.at[c, one], sum_recv.at[0, c]).start()
+        for t in range(1, 4):
+            to = (one + t) % 4
+            remote(
+                dw_tx.at[c, rows(to, 64)], rx_one.at[c, one],
+                sum_send.at[0, c], sum_recv.at[0, c], device(to, two),
+            ).start()
+
+    def second_sums(c):
+        one, two, device = axes(c)
+        arrived(rx_one.at[c], sum_recv.at[0, c])
+        tx_two[c] = jnp.sum(rx_one[c].astype(F32), axis=0).astype(BF16)
+        pltpu.make_async_copy(tx_two.at[c, rows(two, 16)], rx_two.at[c, two], sum_recv.at[1, c]).start()
+        for t in range(1, 4):
+            to = (two + t) % 4
+            remote(
+                tx_two.at[c, rows(to, 16)], rx_two.at[c, two],
+                sum_send.at[1, c], sum_recv.at[1, c], device(one, to),
+            ).start()
+
+    def first_back(c):
+        one, two, device = axes(c)
+        arrived(rx_two.at[c], sum_recv.at[1, c])
+        sum_tx[c] = jnp.sum(rx_two[c].astype(F32), axis=0).astype(BF16)
+        place = dw_sum.at[c, rows(4 * one + two, 16)]
+        pltpu.make_async_copy(sum_tx.at[c], place, sum_recv.at[2, c]).start()
+        for t in range(1, 4):
+            remote(
+                sum_tx.at[c], place, sum_send.at[2, c], sum_recv.at[2, c], device(one, (two + t) % 4)
+            ).start()
+
+    def second_back(c):
+        one, two, device = axes(c)
+        place = dw_sum.at[c, rows(one, 64)]
+        arrived(place, sum_recv.at[2, c])
+        for t in range(1, 4):
+            remote(place, place, sum_send.at[3, c], sum_recv.at[3, c], device((one + t) % 4, two)).start()
+
+    def last_sums():
+        pltpu.make_async_copy(dw_tx.at[LAST, rows(s, 16)], dw_rx.at[s], last_recv.at[0]).start()
 
         @pl.loop(1, SP)
         def _(i):
-            remote(sum_tx.at[c], place, ag_send.at[c], ag_recv.at[c], ((s + i) % SP, d)).start()
-
-    @pl.loop(0, CHUNKS)
-    def _(c):
+            to = (s + i) % SP
+            remote(
+                dw_tx.at[LAST, rows(to, 16)], dw_rx.at[s], last_send.at[0], last_recv.at[0], (to, d)
+            ).start()
+
+    def last_back():
+        arrived(dw_rx, last_recv.at[0])
+        sum_tx[LAST] = jnp.sum(dw_rx[...].astype(F32), axis=0).astype(BF16)
+        place = dw_sum.at[LAST, rows(s, 16)]
+        pltpu.make_async_copy(sum_tx.at[LAST], place, last_recv.at[1]).start()
+
+        @pl.loop(1, SP)
+        def _(i):
+            remote(
+                sum_tx.at[LAST], place, last_send.at[1], last_recv.at[1], ((s + i) % SP, d)
+            ).start()
+
+    def follow_up(i):
+        for n, work in enumerate((second_sums, first_back, second_back)):
+            c = i - 1 - n
+
+            if not isinstance(c, int):
+
+                @pl.when(jnp.logical_and(c >= 0, c < LAST))
+                def _():
+                    work(c)
+
+            elif c < LAST:
+                work(c)
+
+    def gathered(c):
         for n, j in enumerate((left, right, across)):
             arrived(piece(j, c), dk_recv.at[j, c])
             pass_on(j, c, dk_fwd.at[n, c], sibling)
@@ -302,27 +394,19 @@
             arrived(piece(far, c), dk_recv.at[far, c])
         part = dk_all[:, :, col(c, CHUNK)].reshape(DPN * BLOCK, CHUNK)
         dw_tx[c] = dot(xt[...], part, 1, 0).astype(BF16)
-        pltpu.make_async_copy(
-            dw_tx.at[c, pl.ds(pl.multiple_of(16 * s, 16), 16), :], dw_rx.at[c, s], rs_recv.at[c]
-        ).start()
-
-        @pl.loop(1, SP)
-        def _(i):
-            to = (s + i) % SP
-            remote(
-                dw_tx.at[c, pl.ds(pl.multiple_of(16 * to, 16), 16), :], dw_rx.at[c, s],
-                rs_send.at[c], rs_recv.at[c], (to, d),
-            ).start()
-
+        return part
+
+    @pl.loop(0, LAST)
+    def _(c):
+        part = gathered(c)
+        first_sums(c)
         dx_acc[...] += dot(part, w_all[:, col(c, CHUNK)], 1, 1)
-
-        @pl.when(c > 0)
-        def _():
-            sum_chunk(c - 1)
-
-    for j in range(DPN):
-        dx_st[j] = dx_acc[BLOCK * j : BLOCK * (j + 1), :].astype(BF16)
+        follow_up(c)
+
+    part = gathered(LAST)
+    last_sums()
     columns = dx_ref.at[:, col(d, 256)]
+    dx_st[...] = (dx_acc[...] + dot(part, w_all[:, col(LAST, CHUNK)], 1, 1)).astype(BF16).reshape(DPN, BLOCK, 256)
     pltpu.make_async_copy(dx_st.at[d], columns, dx_recv.at[d]).start()
 
     @pl.loop(1, DPN)
@@ -330,7 +414,10 @@
         to = (d + i) % DPN
         remote(dx_st.at[to], columns, dx_send.at[to], dx_recv.at[d], (s, to)).start()
 
-    sum_chunk(CHUNKS - 1)
+    follow_up(LAST)
+    follow_up(CHUNKS)
+    last_back()
+    follow_up(CHUNKS + 1)
 
     @pl.loop(0, GROUP)
     def _(h):
@@ -371,11 +458,21 @@
             arrived(own, dk_send.at[t, c])
         for t in range(3):
             arrived(own, dk_fwd.at[t, c])
-        most = dw_rx.at[c, pl.ds(0, SP - 1)]
-        arrived(most, rs_send.at[c])
-        arrived(most, ag_send.at[c])
-        arrived(dw_sum.at[:, col(c, CHUNK)], ag_recv.at[c])
-        dw_ref[:, col(c, CHUNK)] = dw_sum[:, col(c, CHUNK)].astype(F32)
+
+    @pl.loop(0, LAST)
+    def _(c):
+        arrived(rx_one.at[c, pl.ds(0, 3)], sum_send.at[0, c])
+        arrived(rx_two.at[c, pl.ds(0, 3)], sum_send.at[1, c])
+        arrived(rx_two.at[c, pl.ds(0, 3)], sum_send.at[2, c])
+        three = dw_sum.at[c, pl.ds(0, 192)]
+        arrived(three, sum_send.at[3, c])
+        arrived(three, sum_recv.at[3, c])
+        dw_ref[:, col(c, CHUNK)] = dw_sum[c].astype(F32)
+
+    for n in range(2):
+        arrived(dw_rx.at[pl.ds(0, SP - 1)], last_send.at[n])
+    arrived(dw_sum.at[LAST], last_recv.at[1])
+    dw_ref[:, col(LAST, CHUNK)] = dw_sum[LAST].astype(F32)
 
 
 def write_out(*refs):
@@ -410,11 +507,13 @@
             v_((8, BLOCK, DK), BF16), v_((8, BLOCK, DK), BF16), v_((8, BLOCK, DV), BF16),
             v_((8, BLOCK, D), BF16), v_((8, BLOCK, 256), BF16), v_((8 * BLOCK, 256), F32),
             v_((256, 8 * BLOCK), BF16), v_((CHUNKS, 256, CHUNK), BF16),
-            v_((CHUNKS, 16, 16, CHUNK), BF16), v_((CHUNKS, 16, CHUNK), BF16), v_((256, D), BF16),
+            v_((LAST, 4, 64, CHUNK), BF16), v_((LAST, 64, CHUNK), BF16), v_((LAST, 4, 16, CHUNK), BF16),
+            v_((16, 16, CHUNK), BF16),
+            v_((CHUNKS, 16, CHUNK), BF16), v_((CHUNKS, 256, CHUNK), BF16),
             dma((4, 8)), dma((4, 8)), dma((2,)), dma((2,)), dma((8,)), dma((8,)), dma,
             dma((2,)), dma((2,)), dma((3, 8)), dma((3, 8)),
             dma((4, CHUNKS)), dma((3, CHUNKS)), dma((8, CHUNKS)), dma((8,)), dma((8,)),
-            dma((CHUNKS,)), dma((CHUNKS,)), dma((CHUNKS,)), dma((CHUNKS,)),
+            dma((4, LAST)), dma((4, LAST)), dma((2,)), dma((2,)),
         ],
         compiler_params=pltpu.CompilerParams(
             collective_id=0, has_side_effects=True, vmem_limit_bytes=58 * 1024 * 1024

time: 105 us -> 101 us (0.962)
  Pallas kernels: 104 us -> 100 us
    pallas_call x1, Pallas kernels: 101 us -> 98.3 us  [step(): pl.pallas_call(kernel, out_shape=(v_((BLOCK, 2048), BF16), v_((BLOCK, 409...]
where the time goes in v3:
time: 101 us
  Pallas kernels  100 us (99%)
    pallas_call x1, Pallas kernels, step(): pl.pallas_call(kernel, out_shape=(v_((BLOCK, 2048), BF16), v_((BLOCK, 409...  98.3 us
    pallas_call x1, Pallas kernels, step(): pl.pallas_call(write_out, out_shape=tuple((pltpu.HBM(a.shape, a.dtype) fo...  2.05 us

profile of v3, /device:TPU:1, one launch (start us, length us, event | category | flops | bytes accessed | tf_op | source)
XLA Modules:
  0.0 101.0 jit_solution(4837259806999566811)
XLA Ops:
  0.6 98.3 %shard_map.102 = (bf16[128,2048]{1,0:T(8,128)(2,1)S(1)}, bf16[128,4096]{1,0:T(8,128)(2,1)S(1)}, bf16[128,2048]{1,0:T(8,128)(2,1)S(1)}, f32[256,2048]{1,0:T(8,128)S(1)}) custom-call(bf16[128,2048]{1,0:T(8,128)(2,1)} %bitcast.11, bf16[128,2048]{1,0:T(8,128)(2,1)} %bitcast.12, bf16[128,2048]{1,0:T(8,128)(2,1)} %bitcast.13, bf16[128,4096]{1,0:T(8,128)(2,1)} %bitcast.9, ...), custom_call_target="tpu_custom_call" | custom-call | tf_op jit(solution)/shard_map/pallas_call | solution.py:492
  99.0 2.0 %shard_map.103 = (bf16[128,2048]{1,0:T(8,128)(2,1)}, bf16[128,4096]{1,0:T(8,128)(2,1)}, bf16[128,2048]{1,0:T(8,128)(2,1)}, f32[256,2048]{1,0:T(8,128)}) custom-call(bf16[128,2048]{1,0:T(8,128)(2,1)S(1)} %get-tuple-element.12.refs_0_, bf16[128,4096]{1,0:T(8,128)(2,1)S(1)} %get-tuple-element.13.refs_1_, bf16[128,2048]{1,0:T(8,128)(2,1)S(1)} %get-tuple-element.14.refs_2_, ...), custom_call_target="tpu_custom_call" | custom-call | tf_op jit(solution)/shard_map/pallas_call | solution.py:522
